TPU v7x, 1024 devices: a whole 4x8x16 slice. The times are simulated.
1024 devices in a mesh: row: 32 (over z, core), col: 32 (over y, x).
Axes of the slice: x: 4, y: 8, z: 16, core: 2. Of those that a mesh axis runs over, the one named last changes fastest.
Arguments:
- mix_input: bfloat16 [32, 8192, 1024], P('col', 'row'), may hold values from -6 to 6
- gate_logits: bfloat16 [32, 8192, 2048], P('col', 'row'), may hold values from -8 to 8
- w_proj: bfloat16 [1024, 2048], P('col'), may hold values from -0.1875 to 0.1875
Outputs:
- mixed: bfloat16 [32, 8192, 2048], P('col', 'row')
All inputs are finite; a program needn't handle non-finite values.
Results may differ from a plain program's by a relative error of at most 0.0049.
Values may be sent and summed in bfloat16 or wider, within the bound.
A program may use at most 32 MiB of HBM per device.

v0:
```python
import math

import jax
import jax.numpy as jnp
from jax import lax
from jax.sharding import Mesh
from jax.sharding import PartitionSpec as P

GROUP = 256
GROUPS = 4
POS_INNER = 128
ROW = ("row_0", "row_1")
COL = ("col_0", "col_1")


highest = lax.Precision.HIGHEST


def split_up(value, dim, peers):
    dims = value.shape
    parts = value.reshape(*dims[:dim], peers, dims[dim] // peers, *dims[dim + 1 :])
    return jnp.moveaxis(parts, dim, 0)


def in_order(parts, dim):
    parts = jnp.moveaxis(parts, 0, dim)
    dims = parts.shape
    return parts.reshape(*dims[:dim], dims[dim] * dims[dim + 1], *dims[dim + 2 :])


def exchange_in_order(parts, axes, turns):
    inside = parts.shape[1:]
    out = parts.reshape(*(lax.axis_size(a) for a in axes), *inside)
    for k in turns:
        out = lax.all_to_all(out, axes[k], k, k, tiled=True)
    return out.reshape(-1, *inside)


def exchange_by_chip(value, groups, turns, split_dim, concat_dim):
    peers = lax.axis_size(groups[0]) * lax.axis_size(groups[1])
    parts = split_up(value, split_dim, peers)
    return in_order(exchange_in_order(parts, groups, turns), concat_dim)


def gathered_by_axis(value, axes, dim):
    out = value
    for number in range(len(axes) - 1, -1, -1):
        out = lax.all_gather(out, axes[number], axis=dim, tiled=True)
    return out


def tables(rows_in, cols_out, period):
    left_index = jnp.arange(rows_in, dtype=jnp.int32)[:, None]
    right_index = jnp.arange(cols_out, dtype=jnp.int32)[None, :]
    angles = (left_index * right_index % period).astype(jnp.float32) * (2.0 * math.pi / period)
    return (jnp.cos(angles), jnp.sin(angles))


def half_tables(group_size):
    index_row = jnp.arange(group_size, dtype=jnp.int32)
    frequency = jnp.where(index_row == 1, group_size // 2, index_row // 2)
    is_cosine = jnp.logical_or(index_row % 2 == 0, index_row == 1)
    channel = jnp.arange(group_size, dtype=jnp.int32)[:, None]
    angles = (channel * frequency[None, :] % group_size).astype(jnp.float32) * (
        2.0 * math.pi / group_size
    )
    return jnp.where(is_cosine[None, :], jnp.cos(angles), jnp.sin(angles))


def position_transform(values, inner_len):
    length, columns = values.shape
    outer_len = length // inner_len
    blocks = values.reshape(inner_len, outer_len, columns)
    cos_one, sin_one = tables(inner_len, inner_len, inner_len)
    first_re = jnp.einsum("pqc,pk->ckq", blocks, cos_one, precision=highest)
    first_im = -jnp.einsum("pqc,pk->ckq", blocks, sin_one, precision=highest)
    cos_twist, sin_twist = tables(inner_len, outer_len, length)
    second_re = first_re * cos_twist + first_im * sin_twist
    second_im = first_im * cos_twist - first_re * sin_twist
    cos_two, sin_two = tables(outer_len, outer_len, outer_len)
    whole_re = jnp.einsum("ckq,qj->cjk", second_re, cos_two, precision=highest) + jnp.einsum(
        "ckq,qj->cjk", second_im, sin_two, precision=highest
    )
    whole_im = jnp.einsum("ckq,qj->cjk", second_im, cos_two, precision=highest) - jnp.einsum(
        "ckq,qj->cjk", second_re, sin_two, precision=highest
    )
    return (whole_re.reshape(columns, length), whole_im.reshape(columns, length))


def on_device(mix_input, gate_logits, w_proj):
    tokens = mix_input[0]
    tok_count, features = tokens.shape
    row_count = lax.axis_size(ROW)
    length = tok_count * row_count
    norm_factor = 1.0 / math.sqrt(length * GROUP)
    grouped = tokens.astype(jnp.float32).reshape(tok_count, GROUPS, GROUP)
    packed = jnp.einsum("tgc,cm->tgm", grouped, half_tables(GROUP), precision=highest).reshape(
        tok_count, features
    )
    packed_cols = lax.all_to_all(packed, ROW, split_axis=1, concat_axis=0, tiled=True)
    part_re, part_im = position_transform(packed_cols, POS_INNER)
    columns = part_re.shape[0]
    pair_re = part_re.reshape(columns // 2, 2, length)
    pair_im = part_im.reshape(columns // 2, 2, length)
    pair_index = lax.axis_index(ROW) * (columns // 2) + jnp.arange(columns // 2, dtype=jnp.int32)
    special = (pair_index % (GROUP // 2) == 0)[:, None]
    low_half = jnp.where(special, pair_re[:, 0], pair_re[:, 0] + pair_im[:, 1])
    high_half = jnp.where(special, pair_re[:, 1], pair_re[:, 0] - pair_im[:, 1])
    paired = (
        jnp.stack([low_half, high_half], axis=1).reshape(columns, length) * norm_factor
    ).astype(jnp.bfloat16)
    returned = exchange_by_chip(paired, ("row_0", "row_1"), (1, 0), 1, 0)
    pair_grid = returned.reshape(GROUPS, GROUP // 2, 2, tok_count)
    spectrum = jnp.concatenate(
        [pair_grid[:, :, 0], pair_grid[:, :1, 1], jnp.flip(pair_grid[:, 1:, 1], axis=1)], axis=1
    ).reshape(features, tok_count)
    projected = lax.dot_general(
        spectrum,
        gathered_by_axis(w_proj, COL, 0),
        (((0,), (0,)), ((), ())),
        preferred_element_type=jnp.float32,
    )
    gate_open = jax.nn.sigmoid(gate_logits[0].astype(jnp.float32))
    return (gate_open * projected).astype(jnp.bfloat16)[None]


def solution(mesh):
    split = Mesh(mesh.devices.reshape(16, 2, 8, 4), ("row_0", "row_1", "col_0", "col_1"))
    placed = (P(COL, ROW, None), P(COL, ROW, None), P(COL, None))
    return jax.shard_map(
        on_device, mesh=split, in_specs=placed, out_specs=P(COL, ROW, None), check_vma=False
    )
```

profile of v0, /device:TPU:64, one launch (start us, length us, event | category | flops | bytes accessed | tf_op | source)
XLA Modules:
  0.0 159.7 jit_solution(1690643968074354538)
XLA Ops:
  6.5 1.4 reshape.122
  8.0 0.0 copy-start.1
  8.0 2.7 %fusion.11 = f32[256,256,4]{1,0,2:T(8,128)} fusion(bf16[256,4,256]{2,1,0:T(4,128)(2,1)S(1)} %reshape.122, s32[256]{0:T(256)S(1)} %fusion.69, pred[256]{0:T(512)(128)(4,1)S(1)} %compare_or_fusion), kind=kOutput, calls=%fused_computation.21 | convolution fusion | flops 806289408 | bytes 1574144 | tf_op jit(solution)/shard_map/tgc,cm->tgm/dot_general | solution.py:97
  10.7 18.6 %all-to-all-start = ((f32[256,32,32]{0,2,1:T(8,128)}), f32[256,32,32]{0,2,1:T(8,128)S(1)}, u32[]{:S(2)}, u32[]{:S(2)}) async-start(f32[256,32,32]{0,2,1:T(8,128)} %bitcast.5), calls=%async_computation | async-start | bytes 2097152 | tf_op jit(solution)/shard_map/all_to_all | solution.py:100
  29.2 0.0 all-gather.2.cloned.1.call-start
  29.3 14.1 %all_gather.6 = bf16[128,2048]{1,0:T(8,128)(2,1)} all-gather(bf16[32,2048]{1,0:T(8,128)(2,1)S(1)} %copy-done.1), channel_id=1, replica_groups=mesh['row_0'=16,'row_1'=2,'col_0'=8,'col_1'=4] {'col_1'}, dimensions={0}, use_global_device_ids=true | all-gather | bytes 655360 | tf_op jit(solution)/shard_map/all_gather | solution.py:48
  43.3 0.0 all-gather.2.cloned.1.call-update
  43.4 0.1 fusion.61
  43.5 39.8 %all-to-all-done = f32[256,32,32]{0,2,1:T(8,128)S(1)} async-done(((f32[256,32,32]{0,2,1:T(8,128)}), f32[256,32,32]{0,2,1:T(8,128)S(1)}, u32[]{:S(2)}, u32[]{:S(2)}) %all-to-all-start) | async-done | bytes 1048608 | tf_op jit(solution)/shard_map/all_to_all | solution.py:100
  83.4 0.6 copy.34
  84.0 0.3 reshape.123
  84.3 1.3 copy-done
  85.6 3.5 %convolution_negate_fusion = f32[128,64,32]{0,1,2:T(8,128)S(1)} fusion(f32[128,64,32]{1,0,2:T(8,128)S(1)} %reshape.123), kind=kOutput, calls=%fused_computation.7 | convolution fusion | flops 403144704 | bytes 2097152 | tf_op jit(solution)/shard_map/pqc,pk->ckq/dot_general | solution.py:76
  89.1 5.1 %fusion.36 = f32[128,64,32]{0,1,2:T(8,128)S(1)} fusion(f32[128,64,32]{1,0,2:T(8,128)} %copy-done), kind=kOutput, calls=%fused_computation.51 | convolution fusion | flops 402882560 | bytes 2097152 | tf_op jit(solution)/shard_map/pqc,pk->ckq/dot_general | solution.py:75
  94.2 1.2 fusion.9
  95.4 2.1 %fusion.3 = f32[32,64,128]{2,1,0:T(8,128)} fusion(f32[64,32,128]{2,0,1:T(8,128)S(1)} %fusion.9, f32[128,64,32]{0,1,2:T(8,128)S(1)} %fusion.36, f32[128,64,32]{0,1,2:T(8,128)S(1)} %convolution_negate_fusion, f32[128,64]{0,1:T(8,128)S(1)} %get-tuple-element.7, f32[128,64]{0,1:T(8,128)S(1)} %get-tuple-element.8), kind=kOutput, calls=%fused_computation.6 | convolution fusion | flops 202432512 | bytes 4259840 | tf_op jit(solution)/shard_map/ckq,qj->cjk/dot_general | solution.py:81
  97.6 1.8 %reshape_reshape.6 = f32[16,2,8192]{2,1,0:T(2,128)S(1)} reshape(f32[32,64,128]{2,1,0:T(8,128)} %fusion.3) | data formatting | bytes 2097152 | tf_op jit(solution)/shard_map/reshape;reshape | solution.py:103
  99.4 1.2 fusion.5
  100.6 2.4 %fusion.2 = f32[32,64,128]{2,1,0:T(8,128)} fusion(f32[64,32,128]{2,0,1:T(8,128)S(1)} %fusion.5, f32[128,64,32]{0,1,2:T(8,128)S(1)} %convolution_negate_fusion, f32[128,64,32]{0,1,2:T(8,128)S(1)} %fusion.36, f32[128,64]{0,1:T(8,128)S(1)} %get-tuple-element.7, f32[128,64]{0,1:T(8,128)S(1)} %get-tuple-element.8), kind=kOutput, calls=%fused_computation.4 | convolution fusion | flops 202432512 | bytes 4259840 | tf_op jit(solution)/shard_map/ckq,qj->cjk/dot_general | solution.py:84
  102.9 1.8 %reshape_reshape.7 = f32[16,2,8192]{2,1,0:T(2,128)S(1)} reshape(f32[32,64,128]{2,1,0:T(8,128)} %fusion.2) | data formatting | bytes 2097152 | tf_op jit(solution)/shard_map/reshape;reshape | solution.py:104
  104.8 1.4 broadcast_select_fusion.1
  106.1 1.1 fusion.4
  107.3 0.3 convert_element_type.54
  107.6 0.3 copy.37
  108.0 4.2 %all_to_all.26 = bf16[16,2,32,256]{3,2,0,1:T(8,128)(2,1)S(1)} all-to-all(bf16[16,2,32,256]{3,2,0,1:T(8,128)(2,1)S(1)} %copy.38), channel_id=1, replica_groups=mesh['row_0'=16,'row_1'=2,'col_0'=8,'col_1'=4] {'row_1'}, dimensions={1} | all-to-all | bytes 1048576 | tf_op jit(solution)/shard_map/all_to_all | solution.py:35
  112.2 34.5 %all_to_all.27 = bf16[16,2,32,256]{3,2,1,0:T(8,128)(2,1)S(1)} all-to-all(bf16[16,2,32,256]{3,2,1,0:T(8,128)(2,1)S(1)} %copy.39), channel_id=1, replica_groups=mesh['row_0'=16,'row_1'=2,'col_0'=8,'col_1'=4] {'row_0'}, dimensions={0} | all-to-all | bytes 1048576 | tf_op jit(solution)/shard_map/all_to_all | solution.py:35
  146.7 0.2 reshape_reshape_reshape.3
  146.9 0.6 slice.32
  147.5 0.5 rev.4
  148.1 0.1 pad_maximum_fusion
  148.1 0.0 all-gather.2.cloned.1.call-done
  148.2 4.6 %fusion.1 = bf16[1,256,2048]{2,1,0:T(8,128)(2,1)} fusion(bf16[1024,256]{1,0:T(8,128)(2,1)S(1)} %bitcast.67, bf16[1024,2048]{1,0:T(8,128)(2,1)} %all-gather.2.cloned.1.call-done, bf16[1,256,2048]{2,1,0:T(8,128)(2,1)S(1)} %copy-done.2), kind=kOutput, calls=%fused_computation.2 | convolution fusion | flops 1076887552 | bytes 6815744 | tf_op jit(solution)/shard_map/dot_general | solution.py:117
  (12 shorter events, 0.2 us)
Async XLA Ops:
  8.0 21.3 %copy-start.1 = (bf16[32,2048]{1,0:T(8,128)(2,1)S(1)}, bf16[32,2048]{1,0:T(8,128)(2,1)}, u32[]{:S(2)}) copy-start(bf16[32,2048]{1,0:T(8,128)(2,1)} %param.5) | copy-start | bytes 393220
  10.7 72.7 %all-to-all-start = ((f32[256,32,32]{0,2,1:T(8,128)}), f32[256,32,32]{0,2,1:T(8,128)S(1)}, u32[]{:S(2)}, u32[]{:S(2)}) async-start(f32[256,32,32]{0,2,1:T(8,128)} %bitcast.5), calls=%async_computation | async-start | bytes 2097152 | tf_op jit(solution)/shard_map/all_to_all | solution.py:100
  29.2 118.9 %all-gather.2.cloned.1.call-start = ((), (), s32[]{:S(2)}) async-start(), calls=%async_computation.3 | async-start | bytes 4718592 | tf_op jit(solution)/shard_map/all_gather | solution.py:48
  84.3 1.3 copy-start
  146.9 1.3 copy-start.2
Sparse Core Ops, SparseCore 0:
  43.5 62.4 all-gather.1
where the time goes:
time: 160 us
  blocking collectives  52.7 us (33%)
  waiting for transfers between devices  39.9 us (25%)
  matrix products  22.7 us (14%)
  starting transfers between devices  18.6 us (12%)
  between operations  13.6 us (8%)
  local copies, waits for them, and re-layouts  9.37 us (6%)
  other arithmetic  2.75 us (2%)
    all_to_all x1, waiting for transfers between devices, on_device(): lax.all_to_all(packed, ROW, split_axis=1, concat_axis=0, tiled=True)  39.8 us
    all_to_all x2, blocking collectives, exchange_in_order(): out = lax.all_to_all(out, axes[k], k, k, tiled=True)  38.7 us
    all_to_all x1, starting transfers between devices, on_device(): lax.all_to_all(packed, ROW, split_axis=1, concat_axis=0, tiled=True)  18.6 us
    all_gather x1, blocking collectives, gathered_by_axis(): out = lax.all_gather(out, axes[number], axis=dim, tiled=True)  14.1 us
    dot_general x1, matrix products, position_transform(): first_re = jnp.einsum('pqc,pk->ckq', blocks, cos_one, precision=highest)  5.11 us
    dot_general x1, matrix products, on_device(): lax.dot_general(spectrum, gathered_by_axis(w_proj, COL, 0), (((0,), (0,))...  4.64 us
    dot_general x1, matrix products, position_transform(): first_im = -jnp.einsum('pqc,pk->ckq', blocks, sin_one, precision=highest)  3.49 us
  transfers between devices with their start and end apart: 2, of which 1 were waited for; matrix products, arithmetic and copies ran while one was open for 16% of the time, Pallas kernels for 0%

commit v1 on v0

v1 whole, which is shorter than its diff:
```python
import math

import jax
import jax.numpy as jnp
import numpy as np
from jax import lax
from jax.experimental import pallas as pl
from jax.experimental.pallas import tpu as pltpu
from jax.sharding import Mesh
from jax.sharding import PartitionSpec as P

TOKENS = 256
GROUP = 256
LENGTH = 8192
PEERS = 32
ROWS = 16
CHUNKS = 2
Z, CORES, Y, X = 16, 2, 8, 4
HALF = 1024
F32, BF16 = jnp.float32, jnp.bfloat16
BY_MESH = pl.DeviceIdType.MESH
AXES = ("z", "core", "y", "x")


def high_low(table):
    high = table.astype(np.float32).astype(BF16)
    low = (table - high.astype(np.float64)).astype(np.float32).astype(BF16)
    return high, low


def channel_table():
    row = np.arange(GROUP)
    pair = 8 * (row // 16) + row % 8
    imaginary = row // 8 % 2 == 1
    channel = np.arange(GROUP)[None, :]
    angle = 2.0 * np.pi * ((pair[:, None] * channel) % GROUP) / GROUP
    table = np.where(imaginary[:, None], -np.sin(angle), np.cos(angle))
    half_turn = np.where(np.arange(GROUP) % 2 == 0, 1.0, -1.0)
    table[8] = half_turn
    return np.stack(high_low(table))


def position_table():
    t = np.arange(TOKENS)[:, None]
    lane = np.arange(TOKENS)[None, :]
    j = 8 * (lane % 32) + lane // 32
    angle = 2.0 * np.pi * ((t * j) % TOKENS) / TOKENS
    table = np.concatenate([np.cos(angle), np.sin(angle)], 0) / math.sqrt(LENGTH * GROUP)
    return np.stack(high_low(table))


def twist_table():
    angle = 2.0 * np.pi * np.arange(PEERS)[:, None] * np.arange(TOKENS)[None, :] / LENGTH
    return np.stack([np.cos(angle), -np.sin(angle)]).astype(np.float32)


def order_table():
    row = np.arange(GROUP)
    pair = 8 * (row // 16) + row % 8
    upper = row // 8 % 2 == 1
    channel = np.where(upper, np.where(pair == 0, 128, GROUP - pair), pair)
    return (channel[:, None] == np.arange(GROUP)[None, :]).astype(np.float32).astype(BF16)


def times_root(re, im, k, n):
    if k == 0:
        return re, im
    if 4 * k == n:
        return im, -re
    if 8 * k == n:
        h = math.sqrt(0.5)
        return (re + im) * h, (im - re) * h
    if 8 * k == 3 * n:
        h = math.sqrt(0.5)
        return (im - re) * h, (re + im) * -h
    c, s = math.cos(2 * math.pi * k / n), -math.sin(2 * math.pi * k / n)
    return re * c - im * s, re * s + im * c


def fourier(parts):
    n = len(parts)
    if n == 1:
        return parts
    even, odd = fourier(parts[0::2]), fourier(parts[1::2])
    out = [None] * n
    for k in range(n // 2):
        re, im = times_root(*odd[k], k, n)
        out[k] = (even[k][0] + re, even[k][1] + im)
        out[k + n // 2] = (even[k][0] - re, even[k][1] - im)
    return out


def kernel(mix, gate, w_own, chan, posn, twist, order, out, x, gates, chan_v, posn_v, twist_v, order_v, opened,
           w_all, w_ord, send1, recv1, send2, recv2, spec_hi, spec_lo, whole, turned, acc, result,
           load_sem, s1, r1, s2, r2, wx_s, wx_r, plus_s, plus_r, minus_s, minus_r, core_s, core_r, out_sem):
    z, core, y, col = (lax.axis_index(a) for a in AXES)
    me = z * 2 + core
    barrier = pltpu.get_barrier_semaphore()

    def loaded(k, src, dst):
        return pltpu.make_async_copy(src, dst, load_sem.at[k])

    half = pl.ds(pl.multiple_of(core * HALF, HALF), HALF)
    own = y * X + col
    loads = [
        loaded(0, mix.at[0], x),
        loaded(1, chan, chan_v),
        loaded(2, w_own.at[:, half], w_all.at[own, :, half]),
        loaded(3, gate.at[0], gates),
        loaded(4, posn, posn_v),
        loaded(5, twist, twist_v),
        loaded(6, order, order_v),
    ]
    for copy in loads:
        copy.start()

    def greet(d, carry):
        t = lax.rem(me + d, PEERS)
        pl.semaphore_signal(barrier, inc=1, device_id=(t // 2, t % 2, y, col), device_id_type=BY_MESH)
        return carry

    lax.fori_loop(1, PEERS, greet, 0)
    for d in range(1, X):
        pl.semaphore_signal(barrier, inc=1, device_id=(z, core, y, lax.rem(col + d, X)), device_id_type=BY_MESH)
    up, down = lax.rem(y + 1, Y), lax.rem(y + Y - 1, Y)
    for to in (up, down):
        pl.semaphore_signal(barrier, inc=1, device_id=(z, core, to, col), device_id_type=BY_MESH)

    loads[0].wait()
    loads[1].wait()
    for h in range(CHUNKS):
        for g in range(2):
            lanes = pl.ds((2 * h + g) * GROUP, GROUP)
            part = lax.dot_general(chan_v[0], x[:, lanes], (((1,), (1,)), ((), ())), preferred_element_type=F32)
            part = part + lax.dot_general(chan_v[1], x[:, lanes], (((1,), (1,)), ((), ())), preferred_element_type=F32)
            send1[h, pl.ds(16 * g, 16)] = part.astype(BF16).reshape(16, ROWS, TOKENS)
        recv1[h, me] = send1[h, me]
    pl.semaphore_wait(barrier, 31 + 3 + 2)

    def exchange(src, dst, s_sem, r_sem, h):
        def to(tz, tc):
            t = tz * 2 + tc
            pltpu.make_async_remote_copy(
                src.at[h, t], dst.at[h, me], s_sem.at[h], r_sem.at[h], device_id=(tz, tc, y, col), device_id_type=BY_MESH
            ).start()

        def one(i, carry):
            d = 8 - (i + 2) // 4
            k = (i + 2) % 4
            dz = d + (k // 2) * (16 - 2 * d)
            to(lax.rem(z + dz, Z), k % 2)
            return carry

        lax.fori_loop(0, 30, one, 0)
        to(z, 1 - core)

    def landed(buf, sem, h):
        pltpu.make_async_copy(buf.at[h, pl.ds(0, 31)], buf.at[h, pl.ds(0, 31)], sem.at[h]).wait()

    for h in range(CHUNKS):
        exchange(send1, recv1, s1, r1, h)

    loads[2].wait()
    for d in range(1, X):
        pltpu.make_async_remote_copy(
            w_all.at[own, :, half], w_all.at[own, :, half], wx_s, wx_r,
            device_id=(z, core, y, lax.rem(col + d, X)), device_id_type=BY_MESH,
        ).start()

    def block(yb):
        return w_all.at[pl.ds(yb * X, X), :, half]

    def hand_on(yb, to, send, recv):
        pltpu.make_async_remote_copy(
            block(yb), block(yb), send, recv, device_id=(z, core, to, col), device_id_type=BY_MESH
        ).start()

    def to_core(yb, k):
        pltpu.make_async_remote_copy(
            block(yb), block(yb), core_s.at[k], core_r.at[k], device_id=(z, 1 - core, y, col), device_id_type=BY_MESH
        ).start()

    def bytes_of(yb, sem):
        return pltpu.make_async_copy(block(yb), block(yb), sem)

    row3 = w_all.at[pl.ds(0, 3), :, half]
    pltpu.make_async_copy(row3, row3, wx_r).wait()
    hand_on(y, up, plus_s.at[0], plus_r.at[0])
    hand_on(y, down, minus_s.at[0], minus_r.at[0])
    to_core(y, 0)

    def ring(step):
        yb = lax.rem(y + Y - 1 - step, Y)
        bytes_of(yb, plus_r.at[step]).wait()
        if step < 3:
            hand_on(yb, up, plus_s.at[step + 1], plus_r.at[step + 1])
        to_core(yb, 1 + step)
        if step < 3:
            yb = lax.rem(y + 1 + step, Y)
            bytes_of(yb, minus_r.at[step]).wait()
            if step < 2:
                hand_on(yb, down, minus_s.at[step + 1], minus_r.at[step + 1])
            to_core(yb, 5 + step)

    loads[3].wait()

    def open_gate(i, carry):
        rows = pl.ds(pl.multiple_of(i * 16, 16), 16)
        opened[rows, :] = jax.nn.sigmoid(gates[rows, :].astype(F32))
        return carry

    lax.fori_loop(0, TOKENS // 16, open_gate, 0)
    for k in (4, 5, 6):
        loads[k].wait()
    ring(0)

    sub = lax.broadcasted_iota(jnp.int32, (8, 128), 0)
    lane = lax.broadcasted_iota(jnp.int32, (8, 128), 1)
    alone = jnp.logical_and(sub == 0, lax.rem(me, 16) == 0)

    def transform(h):
        def first(i, carry):
            lanes = pl.ds(pl.multiple_of(i * 128, 128), 128)
            lanes_im = pl.ds(pl.multiple_of(i * 128 + TOKENS, 128), 128)
            parts = []
            for r in range(PEERS):
                both = recv1[h, r, :, lanes].astype(F32)
                parts.append((both[:8], both[8:]))
            freq = fourier(parts)
            for k in range(PEERS):
                pr, pi = freq[k]
                mr, mi = freq[(PEERS - k) % PEERS]
                mi = -mi
                lr = jnp.where(alone, (pr + mr) * 0.5, pr)
                li = jnp.where(alone, (pi + mi) * 0.5, pi)
                hr = jnp.where(alone, (pi - mi) * 0.5, mr)
                hi = jnp.where(alone, (mr - pr) * 0.5, mi)
                c = twist_v[0, pl.ds(k, 1), lanes]
                s = twist_v[1, pl.ds(k, 1), lanes]
                re = jnp.concatenate([lr * c - li * s, hr * c - hi * s], 0)
                im = jnp.concatenate([lr * s + li * c, hr * s + hi * c], 0)
                at = pl.ds(k * ROWS, ROWS)
                for val, where in ((re, lanes), (im, lanes_im)):
                    top = val.astype(BF16)
                    spec_hi[at, where] = top
                    spec_lo[at, where] = (val - top.astype(F32)).astype(BF16)
            return carry

        lax.fori_loop(0, 2, first, 0)

        def second(i, carry):
            rows = pl.ds(pl.multiple_of(i * 128, 128), 128)
            top, rest = spec_hi[rows, :], spec_lo[rows, :]
            whole[rows, :] = (
                jnp.dot(top, posn_v[0], preferred_element_type=F32)
                + jnp.dot(rest, posn_v[0], preferred_element_type=F32)
                + jnp.dot(top, posn_v[1], preferred_element_type=F32)
            )
            return carry

        lax.fori_loop(0, 4, second, 0)

        for sign in range(2):
            for part in range(2):
                lanes = pl.ds(part * 128, 128)
                v = [whole[pl.ds(k * ROWS + sign * 8, 8), lanes] for k in range(PEERS)]
                for bit in (1, 2, 4, 8, 16):
                    odd = (lane // bit) % 2 == 1
                    for a in range(PEERS):
                        if a & bit:
                            continue
                        b = a | bit
                        va, vb = v[a], v[b]
                        v[a] = jnp.where(odd, pltpu.roll(vb, bit, 1), va)
                        v[b] = jnp.where(odd, vb, pltpu.roll(va, 128 - bit, 1))
                for r in range(PEERS):
                    turned[r, pl.ds(sign * 8, 8), lanes] = v[r]

        def pack(r, carry):
            send2[h, r] = turned[r].astype(BF16)
            return carry

        lax.fori_loop(0, PEERS, pack, 0)
        recv2[h, me] = send2[h, me]

    landed(recv1, r1, 0)
    transform(0)
    exchange(send2, recv2, s2, r2, 0)
    ring(1)
    ring(2)
    landed(recv1, r1, 1)
    transform(1)
    exchange(send2, recv2, s2, r2, 1)
    ring(3)

    other = pl.ds(pl.multiple_of((1 - core) * HALF, HALF), HALF)
    for k in range(Y):
        theirs = w_all.at[pl.ds(0, X), :, other]
        pltpu.make_async_copy(theirs, theirs, core_r.at[k]).wait()
    for g in range(4):
        def reorder(i, carry):
            lanes = pl.ds(pl.multiple_of(i * 256, 256), 256)
            rows = w_all[pl.ds(g * 8, 8), :, lanes].reshape(GROUP, 256)
            w_ord[pl.ds(g * GROUP, GROUP), lanes] = jnp.dot(order_v[...], rows, preferred_element_type=F32).astype(BF16)
            return carry

        lax.fori_loop(0, 8, reorder, 0)

    landed(recv2, r2, 0)
    spec = recv2[0].reshape(2 * GROUP, TOKENS).T

    def project(i, carry):
        lanes = pl.ds(pl.multiple_of(i * 256, 256), 256)
        acc[:, lanes] = jnp.dot(spec, w_ord[pl.ds(0, 2 * GROUP), lanes], preferred_element_type=F32)
        return carry

    lax.fori_loop(0, 8, project, 0)
    landed(recv2, r2, 1)
    spec_b = recv2[1].reshape(2 * GROUP, TOKENS).T

    def out_copy(i):
        lanes = pl.ds(pl.multiple_of(i * 256, 256), 256)
        return pltpu.make_async_copy(result.at[:, lanes], out.at[0, :, lanes], out_sem.at[i])

    def finish(i, carry):
        lanes = pl.ds(pl.multiple_of(i * 256, 256), 256)
        full = acc[:, lanes] + jnp.dot(spec_b, w_ord[pl.ds(2 * GROUP, 2 * GROUP), lanes], preferred_element_type=F32)
        result[:, lanes] = (opened[:, lanes] * full).astype(BF16)
        out_copy(i).start()
        return carry

    lax.fori_loop(0, 8, finish, 0)

    for h in range(CHUNKS):
        landed(send1, s1, h)
        landed(send2, s2, h)
    pltpu.make_async_copy(row3, row3, wx_s).wait()
    for k in range(4):
        bytes_of(y, plus_s.at[k]).wait()
    for k in range(3):
        bytes_of(y, minus_s.at[k]).wait()
    for k in range(Y):
        bytes_of(y, core_s.at[k]).wait()
    for i in range(8):
        out_copy(i).wait()


def on_device(mix_input, gate_logits, w_proj):
    dma = pltpu.SemaphoreType.DMA
    hbm = pl.BlockSpec(memory_space=pl.ANY)
    vmem = pltpu.VMEM
    return pl.pallas_call(
        kernel,
        out_shape=jax.ShapeDtypeStruct((1, TOKENS, 2048), BF16),
        in_specs=[hbm] * 7,
        out_specs=hbm,
        scratch_shapes=[
            vmem((TOKENS, 1024), BF16),
            vmem((TOKENS, 2048), BF16),
            vmem((2, GROUP, GROUP), BF16),
            vmem((2, 2 * TOKENS, TOKENS), BF16),
            vmem((2, PEERS, TOKENS), F32),
            vmem((GROUP, GROUP), BF16),
            vmem((TOKENS, 2048), F32),
            vmem((32, 32, 2048), BF16),
            vmem((1024, 2048), BF16),
            vmem((CHUNKS, PEERS, ROWS, TOKENS), BF16),
            vmem((CHUNKS, PEERS, ROWS, TOKENS), BF16),
            vmem((CHUNKS, PEERS, ROWS, TOKENS), BF16),
            vmem((CHUNKS, PEERS, ROWS, TOKENS), BF16),
            vmem((PEERS * ROWS, 2 * TOKENS), BF16),
            vmem((PEERS * ROWS, 2 * TOKENS), BF16),
            vmem((PEERS * ROWS, TOKENS), F32),
            vmem((PEERS, ROWS, TOKENS), F32),
            vmem((TOKENS, 2048), F32),
            vmem((TOKENS, 2048), BF16),
            dma((7,)),
            dma((CHUNKS,)), dma((CHUNKS,)), dma((CHUNKS,)), dma((CHUNKS,)),
            dma(()), dma(()),
            dma((4,)), dma((4,)), dma((3,)), dma((3,)),
            dma((Y,)), dma((Y,)),
            dma((8,)),
        ],
        compiler_params=pltpu.CompilerParams(
            collective_id=0, has_side_effects=True, vmem_limit_bytes=60 * 1024 * 1024
        ),
    )(
        mix_input, gate_logits, w_proj,
        jnp.asarray(channel_table()), jnp.asarray(position_table()), jnp.asarray(twist_table()), jnp.asarray(order_table()),
    )


def solution(mesh):
    split = Mesh(mesh.devices.reshape(Z, CORES, Y, X), AXES)
    rows, cols = ("z", "core"), ("y", "x")
    placed = (P(cols, rows, None), P(cols, rows, None), P(cols, None))
    return jax.shard_map(on_device, mesh=split, in_specs=placed, out_specs=P(cols, rows, None), check_vma=False)
```

time: 160 us -> 73.3 us (0.46)
  the two profiles are of different devices: /device:TPU:64 before, /device:TPU:1 now
where the time goes in v1:
time: 73.3 us; the launch traced here: 73.1 us
  Pallas kernels  70.8 us (97%)
  local copies, waits for them, and re-layouts  2.3 us (3%)
    pallas_call x1, Pallas kernels, on_device(): pl.pallas_call(kernel, out_shape=jax.ShapeDtypeStruct((1, TOKENS, 2048),...  70.8 us
    unnamed x1, local copies, waits for them, and re-layouts  2.3 us

profile of v1, /device:TPU:1, one launch (start us, length us, event | category | flops | bytes accessed | tf_op | source)
XLA Modules:
  0.0 73.1 jit_solution(2246613606851441319)
XLA Ops:
  0.0 70.8 %shard_map.73 = bf16[1,256,2048]{2,1,0:T(8,128)(2,1)} custom-call(bf16[1,256,1024]{2,1,0:T(8,128)(2,1)} %mix.1, bf16[1,256,2048]{2,1,0:T(8,128)(2,1)} %gate.1, bf16[32,2048]{1,0:T(8,128)(2,1)} %w_own.1, bf16[2,256,256]{2,1,0:T(8,128)(2,1)} %constant.8.clone.chan, bf16[2,512,256]{2,1,0:T(8,128)(2,1)} %constant.9.clone.posn, ...), custom_call_target="tpu_custom_call" | custom-call | tf_op jit(solution)/shard_map/pallas_call | solution.py:352
  70.8 2.3 %copy.9 = bf16[1,256,2048]{2,1,0:T(8,128)(2,1)} copy(bf16[1,256,2048]{2,1,0:T(8,128)(2,1)} %shard_map.73) | data formatting | bytes 2097152

commit v2 on v1

--- a/solution.py
+++ b/solution.py
@@ -91,8 +91,8 @@
 
 
 def kernel(mix, gate, w_own, chan, posn, twist, order, out, x, gates, chan_v, posn_v, twist_v, order_v, opened,
-           w_all, w_ord, send1, recv1, send2, recv2, spec_hi, spec_lo, whole, turned, acc, result,
-           load_sem, s1, r1, s2, r2, wx_s, wx_r, plus_s, plus_r, minus_s, minus_r, core_s, core_r, out_sem):
+           w_all, w_ord, send1, recv1, send2, recv2, spec_hi, spec_lo, whole, turned, acc,
+           load_sem, s1, r1, s2, r2, wx_s, wx_r, plus_s, plus_r, minus_s, minus_r, core_s, core_r):
     z, core, y, col = (lax.axis_index(a) for a in AXES)
     me = z * 2 + core
     barrier = pltpu.get_barrier_semaphore()
@@ -306,30 +306,20 @@
 
         lax.fori_loop(0, 8, reorder, 0)
 
+    def project(h, rows, final):
+        spec = recv2[h, :, :, rows].reshape(2 * GROUP, -1).T
+        for i in range(4):
+            lanes = pl.ds(i * 512, 512)
+            full = jnp.dot(spec, w_ord[pl.ds(h * 2 * GROUP, 2 * GROUP), lanes], preferred_element_type=F32)
+            if final:
+                out[0, rows, lanes] = (opened[rows, lanes] * (acc[rows, lanes] + full)).astype(BF16)
+            else:
+                acc[rows, lanes] = full
+
     landed(recv2, r2, 0)
-    spec = recv2[0].reshape(2 * GROUP, TOKENS).T
-
-    def project(i, carry):
-        lanes = pl.ds(pl.multiple_of(i * 256, 256), 256)
-        acc[:, lanes] = jnp.dot(spec, w_ord[pl.ds(0, 2 * GROUP), lanes], preferred_element_type=F32)
-        return carry
-
-    lax.fori_loop(0, 8, project, 0)
+    project(0, pl.ds(0, TOKENS), False)
     landed(recv2, r2, 1)
-    spec_b = recv2[1].reshape(2 * GROUP, TOKENS).T
-
-    def out_copy(i):
-        lanes = pl.ds(pl.multiple_of(i * 256, 256), 256)
-        return pltpu.make_async_copy(result.at[:, lanes], out.at[0, :, lanes], out_sem.at[i])
-
-    def finish(i, carry):
-        lanes = pl.ds(pl.multiple_of(i * 256, 256), 256)
-        full = acc[:, lanes] + jnp.dot(spec_b, w_ord[pl.ds(2 * GROUP, 2 * GROUP), lanes], preferred_element_type=F32)
-        result[:, lanes] = (opened[:, lanes] * full).astype(BF16)
-        out_copy(i).start()
-        return carry
-
-    lax.fori_loop(0, 8, finish, 0)
+    project(1, pl.ds(0, TOKENS), True)
 
     for h in range(CHUNKS):
         landed(send1, s1, h)
@@ -341,19 +331,17 @@
         bytes_of(y, minus_s.at[k]).wait()
     for k in range(Y):
         bytes_of(y, core_s.at[k]).wait()
-    for i in range(8):
-        out_copy(i).wait()
 
 
 def on_device(mix_input, gate_logits, w_proj):
     dma = pltpu.SemaphoreType.DMA
-    hbm = pl.BlockSpec(memory_space=pl.ANY)
+    hbm = pl.BlockSpec(memory_space=pltpu.HBM)
     vmem = pltpu.VMEM
     return pl.pallas_call(
         kernel,
         out_shape=jax.ShapeDtypeStruct((1, TOKENS, 2048), BF16),
         in_specs=[hbm] * 7,
-        out_specs=hbm,
+        out_specs=pl.BlockSpec(memory_space=pltpu.VMEM),
         scratch_shapes=[
             vmem((TOKENS, 1024), BF16),
             vmem((TOKENS, 2048), BF16),
@@ -373,20 +361,23 @@
             vmem((PEERS * ROWS, TOKENS), F32),
             vmem((PEERS, ROWS, TOKENS), F32),
             vmem((TOKENS, 2048), F32),
-            vmem((TOKENS, 2048), BF16),
             dma((7,)),
             dma((CHUNKS,)), dma((CHUNKS,)), dma((CHUNKS,)), dma((CHUNKS,)),
             dma(()), dma(()),
             dma((4,)), dma((4,)), dma((3,)), dma((3,)),
             dma((Y,)), dma((Y,)),
-            dma((8,)),
         ],
         compiler_params=pltpu.CompilerParams(
-            collective_id=0, has_side_effects=True, vmem_limit_bytes=60 * 1024 * 1024
+            collective_id=0, has_side_effects=True, vmem_limit_bytes=28 * 1024 * 1024
         ),
     )(
-        mix_input, gate_logits, w_proj,
-        jnp.asarray(channel_table()), jnp.asarray(position_table()), jnp.asarray(twist_table()), jnp.asarray(order_table()),
+        *(
+            pltpu.with_memory_space_constraint(v, pltpu.HBM)
+            for v in (
+                mix_input, gate_logits, w_proj,
+                jnp.asarray(channel_table()), jnp.asarray(position_table()), jnp.asarray(twist_table()), jnp.asarray(order_table()),
+            )
+        )
     )
 
 

time: 73.3 us -> 70 us (0.955)
  Pallas kernels: 70.8 us -> 68.8 us
  local copies, waits for them, and re-layouts: 2.3 us -> 0.97 us
    pallas_call x1, Pallas kernels: 70.8 us -> 68.8 us  [on_device(): pl.pallas_call(kernel, out_shape=jax.ShapeDtypeStruct((1, TOKENS, 2048),...]
    unnamed x1, local copies, waits for them, and re-layouts: 2.3 us -> 0.97 us
where the time goes in v2:
time: 70 us; the launch traced here: 69.8 us
  Pallas kernels  68.8 us (98%)
  local copies, waits for them, and re-layouts  0.97 us (1%)
    pallas_call x1, Pallas kernels, on_device(): pl.pallas_call(kernel, out_shape=jax.ShapeDtypeStruct((1, TOKENS, 2048),...  68.8 us

profile of v2, /device:TPU:1, one launch (start us, length us, event | category | flops | bytes accessed | tf_op | source)
XLA Modules:
  0.0 69.8 jit_solution(5003875834016101481)
XLA Ops:
  0.0 68.8 %shard_map.73 = bf16[1,256,2048]{2,1,0:T(8,128)(2,1)S(1)} custom-call(bf16[1,256,1024]{2,1,0:T(8,128)(2,1)} %mix.1, bf16[1,256,2048]{2,1,0:T(8,128)(2,1)} %gate.1, bf16[32,2048]{1,0:T(8,128)(2,1)} %w_own.1, bf16[2,256,256]{2,1,0:T(8,128)(2,1)} %constant.8.clone.chan, bf16[2,512,256]{2,1,0:T(8,128)(2,1)} %constant.9.clone.posn, ...), custom_call_target="tpu_custom_call" | custom-call | tf_op jit(solution)/shard_map/pallas_call | solution.py:340
  68.8 1.0 %copy.9 = bf16[1,256,2048]{2,1,0:T(8,128)(2,1)} copy(bf16[1,256,2048]{2,1,0:T(8,128)(2,1)S(1)} %shard_map.73) | data formatting | bytes 2097152

commit v3 on v2

--- a/solution.py
+++ b/solution.py
@@ -103,39 +103,39 @@
     half = pl.ds(pl.multiple_of(core * HALF, HALF), HALF)
     own = y * X + col
     loads = [
-        loaded(0, mix.at[0], x),
+        loaded(0, mix.at[0, :, pl.ds(0, 2 * GROUP)], x.at[:, pl.ds(0, 2 * GROUP)]),
         loaded(1, chan, chan_v),
         loaded(2, w_own.at[:, half], w_all.at[own, :, half]),
         loaded(3, gate.at[0], gates),
         loaded(4, posn, posn_v),
         loaded(5, twist, twist_v),
         loaded(6, order, order_v),
+        loaded(7, mix.at[0, :, pl.ds(2 * GROUP, 2 * GROUP)], x.at[:, pl.ds(2 * GROUP, 2 * GROUP)]),
     ]
-    for copy in loads:
-        copy.start()
-
-    def greet(d, carry):
-        t = lax.rem(me + d, PEERS)
-        pl.semaphore_signal(barrier, inc=1, device_id=(t // 2, t % 2, y, col), device_id_type=BY_MESH)
-        return carry
-
-    lax.fori_loop(1, PEERS, greet, 0)
+    for k in (0, 1):
+        loads[k].start()
+
+    for d in (8, 7, 9, 6, 10, 5, 11, 4, 12, 3, 13, 2, 14, 1, 15):
+        tz = lax.rem(z + d, Z)
+        for tc in range(CORES):
+            pl.semaphore_signal(barrier, inc=1, device_id=(tz, tc, y, col), device_id_type=BY_MESH)
+    pl.semaphore_signal(barrier, inc=1, device_id=(z, 1 - core, y, col), device_id_type=BY_MESH)
     for d in range(1, X):
         pl.semaphore_signal(barrier, inc=1, device_id=(z, core, y, lax.rem(col + d, X)), device_id_type=BY_MESH)
     up, down = lax.rem(y + 1, Y), lax.rem(y + Y - 1, Y)
     for to in (up, down):
         pl.semaphore_signal(barrier, inc=1, device_id=(z, core, to, col), device_id_type=BY_MESH)
 
-    loads[0].wait()
-    loads[1].wait()
-    for h in range(CHUNKS):
+    for k in (7, 2, 3, 4, 5, 6):
+        loads[k].start()
+
+    def channels(h):
         for g in range(2):
             lanes = pl.ds((2 * h + g) * GROUP, GROUP)
             part = lax.dot_general(chan_v[0], x[:, lanes], (((1,), (1,)), ((), ())), preferred_element_type=F32)
             part = part + lax.dot_general(chan_v[1], x[:, lanes], (((1,), (1,)), ((), ())), preferred_element_type=F32)
             send1[h, pl.ds(16 * g, 16)] = part.astype(BF16).reshape(16, ROWS, TOKENS)
         recv1[h, me] = send1[h, me]
-    pl.semaphore_wait(barrier, 31 + 3 + 2)
 
     def exchange(src, dst, s_sem, r_sem, h):
         def to(tz, tc):
@@ -157,8 +157,14 @@
     def landed(buf, sem, h):
         pltpu.make_async_copy(buf.at[h, pl.ds(0, 31)], buf.at[h, pl.ds(0, 31)], sem.at[h]).wait()
 
-    for h in range(CHUNKS):
-        exchange(send1, recv1, s1, r1, h)
+    loads[0].wait()
+    loads[1].wait()
+    channels(0)
+    pl.semaphore_wait(barrier, 31 + 3 + 2)
+    exchange(send1, recv1, s1, r1, 0)
+    loads[7].wait()
+    channels(1)
+    exchange(send1, recv1, s1, r1, 1)
 
     loads[2].wait()
     for d in range(1, X):
@@ -361,7 +367,7 @@
             vmem((PEERS * ROWS, TOKENS), F32),
             vmem((PEERS, ROWS, TOKENS), F32),
             vmem((TOKENS, 2048), F32),
-            dma((7,)),
+            dma((8,)),
             dma((CHUNKS,)), dma((CHUNKS,)), dma((CHUNKS,)), dma((CHUNKS,)),
             dma(()), dma(()),
             dma((4,)), dma((4,)), dma((3,)), dma((3,)),

time: 70 us -> 69.6 us (level)
  no operation moved by 1% of the time
where the time goes in v3:
time: 69.6 us; the launch traced here: 69.4 us
  Pallas kernels  68.4 us (98%)
  local copies, waits for them, and re-layouts  0.97 us (1%)
    pallas_call x1, Pallas kernels, on_device(): pl.pallas_call(kernel, out_shape=jax.ShapeDtypeStruct((1, TOKENS, 2048),...  68.4 us

profile of v3, /device:TPU:1, one launch (start us, length us, event | category | flops | bytes accessed | tf_op | source)
XLA Modules:
  0.0 69.4 jit_solution(2376434806127894239)
XLA Ops:
  0.0 68.4 %shard_map.73 = bf16[1,256,2048]{2,1,0:T(8,128)(2,1)S(1)} custom-call(bf16[1,256,1024]{2,1,0:T(8,128)(2,1)} %mix.1, bf16[1,256,2048]{2,1,0:T(8,128)(2,1)} %gate.1, bf16[32,2048]{1,0:T(8,128)(2,1)} %w_own.1, bf16[2,256,256]{2,1,0:T(8,128)(2,1)} %constant.8.clone.chan, bf16[2,512,256]{2,1,0:T(8,128)(2,1)} %constant.9.clone.posn, ...), custom_call_target="tpu_custom_call" | custom-call | tf_op jit(solution)/shard_map/pallas_call | solution.py:346
  68.4 1.0 %copy.9 = bf16[1,256,2048]{2,1,0:T(8,128)(2,1)} copy(bf16[1,256,2048]{2,1,0:T(8,128)(2,1)S(1)} %shard_map.73) | data formatting | bytes 2097152

commit v4 on v3

--- a/solution.py
+++ b/solution.py
@@ -314,8 +314,8 @@
 
     def project(h, rows, final):
         spec = recv2[h, :, :, rows].reshape(2 * GROUP, -1).T
-        for i in range(4):
-            lanes = pl.ds(i * 512, 512)
+        for i in range(2):
+            lanes = pl.ds(i * 1024, 1024)
             full = jnp.dot(spec, w_ord[pl.ds(h * 2 * GROUP, 2 * GROUP), lanes], preferred_element_type=F32)
             if final:
                 out[0, rows, lanes] = (opened[rows, lanes] * (acc[rows, lanes] + full)).astype(BF16)

time: 69.6 us -> 69.6 us (level)
  no operation moved by 1% of the time
where the time goes in v4:
time: 69.6 us; the launch traced here: 69.4 us
  Pallas kernels  68.4 us (98%)
  local copies, waits for them, and re-layouts  0.97 us (1%)
    pallas_call x1, Pallas kernels, on_device(): pl.pallas_call(kernel, out_shape=jax.ShapeDtypeStruct((1, TOKENS, 2048),...  68.4 us

profile of v4, /device:TPU:1, one launch (start us, length us, event | category | flops | bytes accessed | tf_op | source)
XLA Modules:
  0.0 69.4 jit_solution(2376434806127894239)
XLA Ops:
  0.0 68.4 %shard_map.73 = bf16[1,256,2048]{2,1,0:T(8,128)(2,1)S(1)} custom-call(bf16[1,256,1024]{2,1,0:T(8,128)(2,1)} %mix.1, bf16[1,256,2048]{2,1,0:T(8,128)(2,1)} %gate.1, bf16[32,2048]{1,0:T(8,128)(2,1)} %w_own.1, bf16[2,256,256]{2,1,0:T(8,128)(2,1)} %constant.8.clone.chan, bf16[2,512,256]{2,1,0:T(8,128)(2,1)} %constant.9.clone.posn, ...), custom_call_target="tpu_custom_call" | custom-call | tf_op jit(solution)/shard_map/pallas_call | solution.py:346
  68.4 1.0 %copy.9 = bf16[1,256,2048]{2,1,0:T(8,128)(2,1)} copy(bf16[1,256,2048]{2,1,0:T(8,128)(2,1)S(1)} %shard_map.73) | data formatting | bytes 2097152
